TPU v7x, 32 devices: a whole 2x2x4 slice. The times are simulated.
32 devices in a mesh: sp: 8 (over z, y), tp: 4 (over x, core).
Axes of the slice: x: 2, y: 2, z: 4, core: 2. Of those that a mesh axis runs over, the one named last changes fastest.
Arguments:
- residual: bfloat16 [8192, 2048], P('sp'), may hold values from -8 to 8
- query_wide: bfloat16 [8192, 1024], P('sp', 'tp'), may hold values from -6 to 6
- key_wide: bfloat16 [8192, 1024], P('sp', 'tp'), may hold values from -6 to 6
- value_wide: bfloat16 [8192, 2048], P('sp', 'tp'), may hold values from -6 to 6
- decay_wide: bfloat16 [8192, 1024], P('sp', 'tp'), may hold values from -12 to 12
- gate_wide: bfloat16 [8192, 2048], P('sp', 'tp'), may hold values from -6 to 6
- query_narrow: bfloat16 [8192, 512], P('sp', 'tp'), may hold values from -6 to 6
- key_narrow: bfloat16 [8192, 512], P('sp', 'tp'), may hold values from -6 to 6
- value_narrow: bfloat16 [8192, 2048], P('sp', 'tp'), may hold values from -6 to 6
- decay_narrow: bfloat16 [8192, 512], P('sp', 'tp'), may hold values from -12 to 12
- gate_narrow: bfloat16 [8192, 2048], P('sp', 'tp'), may hold values from -6 to 6
- head_gain: float32 [512], replicated, may hold values from 0.1 to 1.9
- out_wide: bfloat16 [2048, 2048], P('tp'), may hold values from -0.125 to 0.125
- out_narrow: bfloat16 [2048, 2048], P('tp'), may hold values from -0.125 to 0.125
- mlp_gain: float32 [2048], replicated, may hold values from 0.1 to 1.9
- up_weight: bfloat16 [2048, 4096], P('sp', 'tp'), may hold values from -0.125 to 0.125
- down_weight: bfloat16 [4096, 2048], P('tp', 'sp'), may hold values from -0.09375 to 0.09375
Outputs:
- layer_out: bfloat16 [8192, 2048], P('sp', 'tp')
All inputs are finite; a program needn't handle non-finite values.
Results may differ from a plain program's by a relative error of at most 0.017.
Values may be sent and summed in bfloat16 or wider, within the bound.
A program may use at most 128 MiB of HBM per device.

v0:
```python
import jax
import jax.numpy as jnp
from jax import lax
from jax.sharding import PartitionSpec as P

HEADS = 4
BLOCK = 64
EPS = 1e-05
DECAY_NORMALIZER = 16.0
HIGHEST = lax.Precision.HIGHEST


def entering(array, axis, join, neutral):
    place = lax.axis_index(axis)
    gathered = jax.tree.map(
        lambda a, kind: lax.all_gather(a.astype(kind), axis),
        array,
        (jnp.bfloat16, jnp.bfloat16, jnp.bfloat16, jnp.bfloat16),
    )
    state = jax.tree.map(lambda a, e: jnp.zeros_like(a) + jnp.asarray(e, a.dtype), array, neutral)

    def one(step, state):
        return join(
            state,
            jax.tree.map(
                lambda a, own: lax.dynamic_index_in_dim(a, step, 0, False).astype(own.dtype),
                gathered,
                array,
            ),
        )

    return lax.fori_loop(0, place, one, state)


def block_pass(queries, keys_in, values_in, log_decay, block_len):
    num_blocks = queries.shape[0] // block_len

    def to_blocks(stacked):
        return stacked.reshape((num_blocks, block_len) + stacked.shape[1:])

    causal = jnp.tril(jnp.ones((block_len, block_len), dtype=bool))
    initial = (
        jnp.zeros((queries.shape[1], queries.shape[2], values_in.shape[2]), jnp.float32),
        jnp.zeros((queries.shape[1], queries.shape[2]), jnp.float32),
    )

    def advance(running, inputs):
        memory, offset = running
        block_q, block_k, block_v, block_g = inputs
        within = jnp.cumsum(block_g, axis=0)
        final_log = within[-1]
        scaled_q = block_q * jnp.exp(within)
        scaled_k = block_k * jnp.exp(-within)
        outside = jnp.einsum("ihd,hde->ihe", scaled_q, memory, precision=HIGHEST)
        scores = jnp.einsum("ihd,jhd->hij", scaled_q, scaled_k, precision=HIGHEST)
        scores = jnp.where(causal[None], scores, 0.0)
        inside = jnp.einsum("hij,jhe->ihe", scores, block_v, precision=HIGHEST)
        decayed_keys = scaled_k * jnp.exp(final_log)[None]
        memory = jnp.exp(final_log)[..., None] * memory + jnp.einsum(
            "jhd,jhe->hde", decayed_keys, block_v, precision=HIGHEST
        )
        carried_q = scaled_q * jnp.exp(offset)[None]
        return ((memory, offset + final_log), (outside + inside, carried_q))

    (memory, totals), (outputs, carried_q) = lax.scan(
        advance,
        initial,
        (to_blocks(queries), to_blocks(keys_in), to_blocks(values_in), to_blocks(log_decay)),
    )
    return (outputs.reshape(values_in.shape), carried_q.reshape(queries.shape), totals, memory)


def prepare(query, key_proj, value, decay, heads_here):
    row_count = query.shape[0]
    key_width = query.shape[1] // heads_here
    queries = query.astype(jnp.float32).reshape(row_count, heads_here, key_width) * key_width ** (
        -0.5
    )
    keys_in = key_proj.astype(jnp.float32).reshape(row_count, heads_here, key_width)
    values_in = value.astype(jnp.float32).reshape(
        row_count, heads_here, value.shape[1] // heads_here
    )
    log_decay = (
        jax.nn.log_sigmoid(decay.astype(jnp.float32)).reshape(row_count, heads_here, key_width)
        / DECAY_NORMALIZER
    )
    return (queries, keys_in, values_in, log_decay)


def finish(outputs, gate, head_gain):
    scale = lax.rsqrt(jnp.mean(jnp.square(outputs), axis=-1, keepdims=True) + EPS)
    gated = (
        outputs * scale * head_gain * jax.nn.silu(gate.astype(jnp.float32).reshape(outputs.shape))
    )
    return gated.reshape(outputs.shape[0], -1).astype(jnp.bfloat16)


def combine_states(earlier, later):
    return (
        earlier[0] + later[0],
        jnp.exp(later[0])[..., None] * earlier[1] + later[1],
        earlier[2] + later[2],
        jnp.exp(later[2])[..., None] * earlier[3] + later[3],
    )


def body(
    residual,
    query_wide,
    key_wide,
    value_wide,
    decay_wide,
    gate_wide,
    query_narrow,
    key_narrow,
    value_narrow,
    decay_narrow,
    gate_narrow,
    head_gain,
    out_wide,
    out_narrow,
    mlp_gain,
    up_weight,
    down_weight,
):
    heads_here = HEADS // lax.axis_size("tp")
    up_whole, down_whole = (
        lax.all_gather(up_weight, "sp", axis=0, tiled=True),
        lax.all_gather(down_weight, "sp", axis=1, tiled=True),
    )
    wq, wk, wv, wg = prepare(query_wide, key_wide, value_wide, decay_wide, heads_here)
    wide_out, wide_q, wide_total, wide_memory = block_pass(wq, wk, wv, wg, BLOCK)
    nq, nk, nv, ng = prepare(query_narrow, key_narrow, value_narrow, decay_narrow, heads_here)
    narrow_out, narrow_q, narrow_total, narrow_memory = block_pass(nq, nk, nv, ng, BLOCK)
    identity = (
        jnp.zeros_like(wide_total),
        jnp.zeros_like(wide_memory),
        jnp.zeros_like(narrow_total),
        jnp.zeros_like(narrow_memory),
    )
    incoming = entering(
        (wide_total, wide_memory, narrow_total, narrow_memory), "sp", combine_states, identity
    )
    wide_out = wide_out + jnp.einsum("ihd,hde->ihe", wide_q, incoming[1], precision=HIGHEST)
    narrow_out = narrow_out + jnp.einsum("ihd,hde->ihe", narrow_q, incoming[3], precision=HIGHEST)
    gated_wide = finish(wide_out, gate_wide, head_gain)
    gated_narrow = finish(narrow_out, gate_narrow, head_gain)
    head_terms = jnp.dot(gated_wide, out_wide, preferred_element_type=jnp.float32) + jnp.dot(
        gated_narrow, out_narrow, preferred_element_type=jnp.float32
    )
    tp_index = lax.axis_index("tp")
    col_count = residual.shape[1] // lax.axis_size("tp")
    full_width = residual.shape[1]
    residual_cols = lax.dynamic_slice_in_dim(residual, tp_index * col_count, col_count, 1)
    mixed_cols = lax.psum_scatter(
        head_terms.astype(jnp.bfloat16), "tp", scatter_dimension=1, tiled=True
    ).astype(jnp.float32)
    stream_cols = (residual_cols.astype(jnp.float32) + mixed_cols).astype(jnp.bfloat16)
    stream_f = stream_cols.astype(jnp.float32)
    squares = lax.psum(jnp.sum(jnp.square(stream_f), axis=1, keepdims=True), "tp")
    gain_cols = lax.dynamic_slice_in_dim(mlp_gain, tp_index * col_count, col_count, 0)
    normed_cols = (stream_f * lax.rsqrt(squares / full_width + EPS) * gain_cols).astype(
        jnp.bfloat16
    )
    normed = lax.all_gather(normed_cols, "tp", axis=1, tiled=True)
    before_activation = jnp.dot(normed, up_whole, preferred_element_type=jnp.float32)
    hidden = jnp.square(jax.nn.relu(before_activation)).astype(jnp.bfloat16)
    down_terms = jnp.dot(hidden, down_whole, preferred_element_type=jnp.float32)
    mlp_cols = lax.psum_scatter(
        down_terms.astype(jnp.bfloat16), "tp", scatter_dimension=1, tiled=True
    ).astype(jnp.float32)
    return (stream_cols.astype(jnp.float32) + mlp_cols).astype(jnp.bfloat16)


def solution(mesh):
    return jax.shard_map(
        body,
        mesh=mesh,
        in_specs=(
            P("sp", None),
            P("sp", "tp"),
            P("sp", "tp"),
            P("sp", "tp"),
            P("sp", "tp"),
            P("sp", "tp"),
            P("sp", "tp"),
            P("sp", "tp"),
            P("sp", "tp"),
            P("sp", "tp"),
            P("sp", "tp"),
            P(),
            P("tp", None),
            P("tp", None),
            P(),
            P("sp", "tp"),
            P("tp", "sp"),
        ),
        out_specs=P("sp", "tp"),
        check_vma=False,
    )
```

profile of v0, /device:TPU:0, one launch (start us, length us, event | category | flops | bytes accessed | tf_op | source)
XLA Modules:
  0.0 591.7 jit_solution(7153783925277661843)
XLA Ops:
  6.6 5.0 reshape.501
  15.4 68.5 %while.51 = (s32[]{:T(128)}, f32[1,128,512]{2,1,0:T(8,128)S(1)}, f32[1,128]{1,0:T(1,128)S(1)}, f32[16,64,1,512]{3,1,2,0:T(8,128)}, f32[16,64,1,128]{3,1,2,0:T(8,...) while((s32[]{:T(128)}, f32[1,128,512]{2,1,0:T(8,128)S(1)}, ...), condition=%wide.region_5.6_spmd.clone, body=%wide.region_3.5_spmd.clone.sunk | while | flops 133005568 | bytes 2333321 | solution.py:65
  84.7 2.7 fusion.81
  87.3 3.3 reshape.486
  91.6 3.3 reshape.487
  95.0 4.9 reshape.499
  99.8 2.0 reshape.498
  103.4 108.7 %while.50 = (s32[]{:T(128)}, f32[1,256,512]{2,1,0:T(8,128)S(1)}, f32[1,256]{1,0:T(1,128)S(1)}, f32[16,64,1,512]{3,1,2,0:T(8,128)}, f32[16,64,1,256]{3,1,2,0:T(8,...) while((s32[]{:T(128)}, f32[1,256,512]{2,1,0:T(8,128)S(1)}, ...), condition=%wide.region_2.3_spmd.clone, body=%wide.region_0.2_spmd.clone.sunk | while | flops 240787968 | bytes 3648133 | solution.py:65
  212.9 3.0 copy.32
  217.2 3.0 copy.34
  221.5 22.3 %all-gather.5 = bf16[8,1,128]{2,1,0:T(2,128)(2,1)S(1)} all-gather(bf16[1,1,128]{2,1,0:T(2,128)(2,1)S(1)} %convert_bitcast_fusion.1), channel_id=4, replica_groups=mesh['sp'=8,'tp'=4] {'sp'}, dimensions={0}, use_global_device_ids=true | all-gather | bytes 2304 | tf_op jit(solution)/shard_map/all_gather | solution.py:16
  243.9 16.7 %all-gather.4 = bf16[8,1,256]{2,1,0:T(2,128)(2,1)S(1)} all-gather(bf16[1,1,256]{2,1,0:T(2,128)(2,1)S(1)} %convert_bitcast_fusion), channel_id=2, replica_groups=mesh['sp'=8,'tp'=4] {'sp'}, dimensions={0}, use_global_device_ids=true | all-gather | bytes 4608 | tf_op jit(solution)/shard_map/all_gather | solution.py:16
  260.6 4.6 all-gather.18.cloned.1.call-done
  265.4 5.6 multiply_reduce_fusion.1
  273.2 2.8 fusion.78
  276.0 5.0 add_convert_fusion
  283.0 56.4 %reduce-scatter.3.cloned.1.call-done = bf16[1024,512]{1,0:T(8,128)(2,1)} async-done(((bf16[1024,2048]{1,0:T(8,128)(2,1)}), bf16[1024,512]{1,0:T(8,128)(2,1)}) %reduce-scatter.3.cloned.1.call-update) | async-done | bytes 1048592 | tf_op jit(solution)/shard_map/reduce_scatter | solution.py:155
  341.4 5.8 psum.7
  348.8 65.5 %all-gather.14.cloned.1.call-done = bf16[2048,1024]{1,0:T(8,128)(2,1)} async-done(((bf16[256,1024]{1,0:T(8,128)(2,1)}), bf16[2048,1024]{1,0:T(8,128)(2,1)}) %all-gather.14.cloned.1.call-update) | async-done | bytes 4194320 | tf_op jit(solution)/shard_map/all_gather | solution.py:128
  414.3 75.1 %all-gather.16.cloned.1.call-done = bf16[1024,2048]{1,0:T(8,128)(2,1)} async-done(((bf16[1024,256]{1,0:T(8,128)(2,1)}), bf16[1024,2048]{1,0:T(8,128)(2,1)}) %all-gather.16.cloned.1.call-update) | async-done | bytes 4194320 | tf_op jit(solution)/shard_map/all_gather | solution.py:129
  489.4 34.1 %all-gather.12.cloned.1.call-done = bf16[1024,2048]{1,0:T(8,128)(2,1)} async-done(((bf16[1024,512]{1,0:T(8,128)(2,1)}), bf16[1024,2048]{1,0:T(8,128)(2,1)}) %all-gather.12.cloned.1.call-update) | async-done | bytes 4194320 | tf_op jit(solution)/shard_map/all_gather | solution.py:165
  523.4 14.4 %convolution_convert_fusion = bf16[1024,2048]{1,0:T(8,128)(2,1)} fusion(bf16[1024,2048]{1,0:T(8,128)(2,1)} %all-gather.16.cloned.1.call-done, bf16[1024,2048]{1,0:T(8,128)(2,1)} %all-gather.12.cloned.1.call-done, bf16[2048,1024]{1,0:T(8,128)(2,1)} %all-gather.14.cloned.1.call-done), kind=kOutput, calls=%fused_computation.91 | convolution fusion | flops 8595177472 | bytes 16777216 | tf_op jit(solution)/shard_map/dot_general | solution.py:168
  537.9 44.5 %reduce-scatter.5.cloned.1.call-done = bf16[1024,512]{1,0:T(8,128)(2,1)} async-done(((bf16[1024,2048]{1,0:T(8,128)(2,1)}), bf16[1024,512]{1,0:T(8,128)(2,1)}) %reduce-scatter.5.cloned.1.call-update) | async-done | bytes 1048592 | tf_op jit(solution)/shard_map/reduce_scatter | solution.py:169
  582.4 2.5 fusion.74
  (423 shorter events, 193.9 us)
Async XLA Ops:
  6.5 266.6 %copy-start = (bf16[512,2048]{1,0:T(8,128)(2,1)S(1)}, bf16[512,2048]{1,0:T(8,128)(2,1)}, u32[]{:S(2)}) copy-start(bf16[512,2048]{1,0:T(8,128)(2,1)} %param.35) | copy-start | bytes 6291460
  6.5 5.0 copy-start.10
  6.5 5.1 copy-start.11
  6.5 254.0 %all-gather.20.cloned.1.call-start = ((), (), s32[]{:S(2)}) async-start(), calls=%async_computation.8 | async-start | bytes 1179648 | tf_op jit(solution)/shard_map/all_gather | solution.py:16
  83.9 6.7 %copy-start.7 = (bf16[1024,256]{1,0:T(8,128)(2,1)S(1)}, bf16[1024,256]{1,0:T(8,128)(2,1)}, u32[]{:S(2)}) copy-start(bf16[1024,256]{1,0:T(8,128)(2,1)} %param.24) | copy-start | bytes 1572868
  84.6 180.5 %all-gather.18.cloned.1.call-start = ((), (), s32[]{:S(2)}) async-start(), calls=%async_computation.7 | async-start | bytes 2359296 | tf_op jit(solution)/shard_map/all_gather | solution.py:16
  91.6 8.2 %copy-start.8 = (bf16[1024,256]{1,0:T(8,128)(2,1)S(1)}, bf16[1024,256]{1,0:T(8,128)(2,1)}, u32[]{:S(2)}) copy-start(bf16[1024,256]{1,0:T(8,128)(2,1)} %param.25) | copy-start | bytes 1572868
  212.9 126.6 %reduce-scatter.3.cloned.1.call-start = ((), (), s32[]{:S(2)}) async-start(), calls=%async_computation.2 | async-start | bytes 5242880 | tf_op jit(solution)/shard_map/reduce_scatter | solution.py:155
  212.9 3.0 copy-start.3
  217.2 3.0 copy-start.4
  265.4 5.7 copy-start.2
  265.4 5.7 copy-start.9
  271.1 2.1 copy-start.6
  271.1 2.1 copy-start.13
  273.2 2.8 copy-start.5
  273.2 2.8 copy-start.12
  281.0 133.2 %all-gather.14.cloned.1.call-start = ((), (), s32[]{:S(2)}) async-start(), calls=%async_computation.4 | async-start | bytes 4718592 | tf_op jit(solution)/shard_map/all_gather | solution.py:128
  281.6 207.7 %all-gather.16.cloned.1.call-start = ((), (), s32[]{:S(2)}) async-start(), calls=%async_computation.5 | async-start | bytes 4718592 | tf_op jit(solution)/shard_map/all_gather | solution.py:129
  282.2 241.2 %all-gather.12.cloned.1.call-start = ((), (), s32[]{:S(2)}) async-start(), calls=%async_computation.3 | async-start | bytes 5242880 | tf_op jit(solution)/shard_map/all_gather | solution.py:165
  348.5 233.9 %reduce-scatter.5.cloned.1.call-start = ((), (), s32[]{:S(2)}) async-start(), calls=%async_computation.6 | async-start | bytes 5242880 | tf_op jit(solution)/shard_map/reduce_scatter | solution.py:169
  537.9 47.0 %copy-start.1 = (bf16[512,2048]{1,0:T(8,128)(2,1)S(1)}, bf16[512,2048]{1,0:T(8,128)(2,1)}, u32[]{:S(2)}) copy-start(bf16[512,2048]{1,0:T(8,128)(2,1)} %param.35) | copy-start | bytes 6291460
Sparse Core Ops, SparseCore 0:
  84.7 43.0 all-gather.19
  213.0 52.1 all-gather.17
  281.2 58.2 reduce-scatter.2
  341.4 72.7 all-gather.13
  416.2 73.1 all-gather.15
  490.8 32.6 all-gather.11
  538.0 44.3 reduce-scatter.4
where the time goes:
time: 596 us; the launch traced here: 592 us
  waiting for transfers between devices  281 us (47%)
  matrix products  95.3 us (16%)
  local copies, waits for them, and re-layouts  83 us (14%)
  other arithmetic  71.2 us (12%)
  blocking collectives  44.8 us (8%)
  between operations  13.8 us (2%)
    all_gather x1, waiting for transfers between devices, body(): lax.all_gather(down_weight, 'sp', axis=1, tiled=True)  75.1 us
    all_gather x1, waiting for transfers between devices, body(): lax.all_gather(up_weight, 'sp', axis=0, tiled=True)  65.5 us
    reduce_scatter x1, waiting for transfers between devices, body(): lax.psum_scatter(head_terms.astype(jnp.bfloat16), 'tp', scatter_dimension...  56.4 us
    reduce_scatter x1, waiting for transfers between devices, body(): lax.psum_scatter(down_terms.astype(jnp.bfloat16), 'tp', scatter_dimension...  44.5 us
    dynamic_slice x48, local copies, waits for them, and re-layouts, block_pass(): lax.scan(advance, initial, (to_blocks(queries), to_blocks(keys_in), to_bl...  41.7 us
    all_gather x2, blocking collectives, entering(): lax.all_gather(a.astype(kind), axis)  39 us
    all_gather x1, waiting for transfers between devices, body(): normed = lax.all_gather(normed_cols, 'tp', axis=1, tiled=True)  34.1 us
    dot_general x32, matrix products, advance(): outside = jnp.einsum('ihd,hde->ihe', scaled_q, memory, precision=HIGHEST)  22.1 us
  transfers between devices with their start and end apart: 7, of which 6 were waited for; matrix products, arithmetic and copies ran while one was open for 24% of the time, Pallas kernels for 0%

commit v1 on v0

--- a/solution.py
+++ b/solution.py
@@ -162,7 +162,12 @@
     normed_cols = (stream_f * lax.rsqrt(squares / full_width + EPS) * gain_cols).astype(
         jnp.bfloat16
     )
-    normed = lax.all_gather(normed_cols, "tp", axis=1, tiled=True)
+    ring = [normed_cols]
+    for hop in range(3):
+        ring.append(lax.ppermute(ring[-1], "tp", [(dev, (dev + 1) % 4) for dev in range(4)]))
+    normed = jnp.roll(
+        jnp.concatenate(ring[::-1], axis=1), (lax.axis_index("tp") + 1) * ring[0].shape[1], axis=1
+    )
     before_activation = jnp.dot(normed, up_whole, preferred_element_type=jnp.float32)
     hidden = jnp.square(jax.nn.relu(before_activation)).astype(jnp.bfloat16)
     down_terms = jnp.dot(hidden, down_whole, preferred_element_type=jnp.float32)

time: 596 us -> 560 us (0.940)
  waiting for transfers between devices: 281 us -> 235 us
  local copies, waits for them, and re-layouts: 83 us -> 92.1 us
    all_gather x1, waiting for transfers between devices: 65.5 us -> 12 us  [body(): lax.all_gather(up_weight, 'sp', axis=0, tiled=True)]
    ppermute x0 -> x3, waiting for transfers between devices: none -> 42.8 us  [body(): lax.ppermute(ring[-1], 'tp', [(dev, (dev + 1) % 4) for dev in range(4)])]
    all_gather x1 -> x0, waiting for transfers between devices: 34.1 us -> none  [body(): normed = lax.all_gather(normed_cols, 'tp', axis=1, tiled=True)]
    unnamed x30 -> x36, local copies, waits for them, and re-layouts: 2.69 us -> 11.8 us
  transfers between devices with their start and end apart: 7 -> 9, of which waited for: 6 -> 8; matrix products, arithmetic and copies ran while one was open for 24% -> 27% of each run, Pallas kernels for 0% -> 0%
where the time goes in v1:
time: 560 us; the launch traced here: 556 us
  waiting for transfers between devices  235 us (42%)
  matrix products  95.3 us (17%)
  local copies, waits for them, and re-layouts  92.1 us (16%)
  other arithmetic  73 us (13%)
  blocking collectives  44.8 us (8%)
  between operations  13.8 us (2%)
    all_gather x1, waiting for transfers between devices, body(): lax.all_gather(down_weight, 'sp', axis=1, tiled=True)  75.1 us
    reduce_scatter x1, waiting for transfers between devices, body(): lax.psum_scatter(head_terms.astype(jnp.bfloat16), 'tp', scatter_dimension...  56.4 us
    ppermute x3, waiting for transfers between devices, body(): lax.ppermute(ring[-1], 'tp', [(dev, (dev + 1) % 4) for dev in range(4)])  42.8 us
    reduce_scatter x1, waiting for transfers between devices, body(): lax.psum_scatter(down_terms.astype(jnp.bfloat16), 'tp', scatter_dimension...  42.7 us
    dynamic_slice x48, local copies, waits for them, and re-layouts, block_pass(): lax.scan(advance, initial, (to_blocks(queries), to_blocks(keys_in), to_bl...  41.7 us
    all_gather x2, blocking collectives, entering(): lax.all_gather(a.astype(kind), axis)  39 us
    dot_general x32, matrix products, advance(): outside = jnp.einsum('ihd,hde->ihe', scaled_q, memory, precision=HIGHEST)  22.1 us
    dot_general x32, matrix products, advance(): inside = jnp.einsum('hij,jhe->ihe', scores, block_v, precision=HIGHEST)  19.4 us
  transfers between devices with their start and end apart: 9, of which 8 were waited for; matrix products, arithmetic and copies ran while one was open for 27% of the time, Pallas kernels for 0%

profile of v1, /device:TPU:0, one launch (start us, length us, event | category | flops | bytes accessed | tf_op | source)
XLA Modules:
  0.0 555.8 jit_solution(17129936158875103754)
XLA Ops:
  6.6 5.0 reshape.501
  15.4 68.5 %while.51 = (s32[]{:T(128)}, f32[1,128,512]{2,1,0:T(8,128)S(1)}, f32[1,128]{1,0:T(1,128)S(1)}, f32[16,64,1,512]{3,1,2,0:T(8,128)}, f32[16,64,1,128]{3,1,2,0:T(8,...) while((s32[]{:T(128)}, f32[1,128,512]{2,1,0:T(8,128)S(1)}, ...), condition=%wide.region_5.6_spmd.clone, body=%wide.region_3.5_spmd.clone.sunk | while | flops 133005568 | bytes 2333321 | solution.py:65
  84.7 2.7 fusion.88
  87.3 3.3 reshape.486
  91.6 3.3 reshape.487
  95.0 4.9 reshape.499
  103.4 108.7 %while.50 = (s32[]{:T(128)}, f32[1,256,512]{2,1,0:T(8,128)S(1)}, f32[1,256]{1,0:T(1,128)S(1)}, f32[16,64,1,512]{3,1,2,0:T(8,128)}, f32[16,64,1,256]{3,1,2,0:T(8,...) while((s32[]{:T(128)}, f32[1,256,512]{2,1,0:T(8,128)S(1)}, ...), condition=%wide.region_2.3_spmd.clone, body=%wide.region_0.2_spmd.clone.sunk | while | flops 240787968 | bytes 3648133 | solution.py:65
  212.9 3.0 copy.32
  217.2 3.0 copy.34
  221.5 22.3 %all-gather.5 = bf16[8,1,128]{2,1,0:T(2,128)(2,1)S(1)} all-gather(bf16[1,1,128]{2,1,0:T(2,128)(2,1)S(1)} %convert_bitcast_fusion.1), channel_id=4, replica_groups=mesh['sp'=8,'tp'=4] {'sp'}, dimensions={0}, use_global_device_ids=true | all-gather | bytes 2304 | tf_op jit(solution)/shard_map/all_gather | solution.py:16
  243.9 16.7 %all-gather.4 = bf16[8,1,256]{2,1,0:T(2,128)(2,1)S(1)} all-gather(bf16[1,1,256]{2,1,0:T(2,128)(2,1)S(1)} %convert_bitcast_fusion), channel_id=2, replica_groups=mesh['sp'=8,'tp'=4] {'sp'}, dimensions={0}, use_global_device_ids=true | all-gather | bytes 4608 | tf_op jit(solution)/shard_map/all_gather | solution.py:16
  260.6 4.6 all-gather.15.cloned.1.call-done
  265.4 5.6 %multiply_reduce_fusion.1 = (f32[1024]{0:T(1024)S(1)}, f32[1024,1,512]{0,2,1:T(8,128)S(1)}) fusion(f32[1024,1,512]{0,2,1:T(8,128)} %copy.32, f32[1024,256]{1,0:T(8,128)} %bitcast.284, f32[1,256,512]{2,1,0:T(8,128)S(1)} %get-tuple-element.190), kind=kOutput, calls=%fused_computation.123 | convolution fusion | flops 1612184576 | bytes 5771264 | tf_op jit(solution)/shard_map/ihd,hde->ihe/dot_general | solution.py:144
  273.2 2.8 fusion.85
  276.0 5.0 add_convert_fusion
  283.0 56.4 %reduce-scatter.3.cloned.1.call-done = bf16[1024,512]{1,0:T(8,128)(2,1)} async-done(((bf16[1024,2048]{1,0:T(8,128)(2,1)}), bf16[1024,512]{1,0:T(8,128)(2,1)}) %reduce-scatter.3.cloned.1.call-update) | async-done | bytes 1048592 | tf_op jit(solution)/shard_map/reduce_scatter | solution.py:155
  341.4 5.8 %psum.7 = f32[1024,1]{0,1:T(1,128)S(1)} all-reduce(f32[1024,1]{0,1:T(1,128)S(1)} %bitcast.297), channel_id=1, replica_groups=mesh['sp'=8,'tp'=4] {'tp'}, use_global_device_ids=true, to_apply=%region_12.13 | all-reduce | flops 1024 | bytes 8192 | tf_op jit(solution)/shard_map/psum | solution.py:160
  347.6 14.2 %collective-permute-done = bf16[1024,512]{1,0:T(8,128)(2,1)S(1)} collective-permute-done((bf16[1024,512]{1,0:T(8,128)(2,1)S(1)}, bf16[1024,512]{1,0:T(8,128)(2,1)S(1)}, u32[]{:S(2)}, u32[]{:S(2)}) %collective-permute-start) | collective-permute-done | bytes 1048608 | tf_op jit(solution)/shard_map/ppermute | solution.py:167
  361.8 14.2 %collective-permute-done.1 = bf16[1024,512]{1,0:T(8,128)(2,1)S(1)} collective-permute-done((bf16[1024,512]{1,0:T(8,128)(2,1)S(1)}, bf16[1024,512]{1,0:T(8,128)(2,1)S(1)}, u32[]{:S(2)}, u32[]{:S(2)}) %collective-permute-start.1) | collective-permute-done | bytes 1048608 | tf_op jit(solution)/shard_map/ppermute | solution.py:167
  376.0 14.3 %collective-permute-done.2 = bf16[1024,512]{1,0:T(8,128)(2,1)} collective-permute-done((bf16[1024,512]{1,0:T(8,128)(2,1)S(1)}, bf16[1024,512]{1,0:T(8,128)(2,1)}, u32[]{:S(2)}, u32[]{:S(2)}) %collective-permute-start.2) | collective-permute-done | bytes 1048608 | tf_op jit(solution)/shard_map/ppermute | solution.py:167
  402.2 12.0 %all-gather.11.cloned.1.call-done = bf16[2048,1024]{1,0:T(8,128)(2,1)} async-done(((bf16[256,1024]{1,0:T(8,128)(2,1)}), bf16[2048,1024]{1,0:T(8,128)(2,1)}) %all-gather.11.cloned.1.call-update) | async-done | bytes 4194320 | tf_op jit(solution)/shard_map/all_gather | solution.py:128
  414.2 75.1 %all-gather.13.cloned.1.call-done = bf16[1024,2048]{1,0:T(8,128)(2,1)} async-done(((bf16[1024,256]{1,0:T(8,128)(2,1)}), bf16[1024,2048]{1,0:T(8,128)(2,1)}) %all-gather.13.cloned.1.call-update) | async-done | bytes 4194320 | tf_op jit(solution)/shard_map/all_gather | solution.py:129
  489.3 14.4 %convolution_convert_fusion = bf16[1024,2048]{1,0:T(8,128)(2,1)} fusion(bf16[1024,2048]{1,0:T(8,128)(2,1)} %all-gather.13.cloned.1.call-done, bf16[2048,1024]{1,0:T(8,128)(2,1)} %all-gather.11.cloned.1.call-done, bf16[1024,4096]{1,0:T(8,128)(2,1)} %constant_dynamic-update-slice_fusion, s32[]{:T(128)S(6)} %select_n.54), kind=kOutput, calls=%fused_computation.93 | convolution fusion | flops 8595177472 | bytes 16777220 | tf_op jit(solution)/shard_map/dot_general | solution.py:173
  503.7 42.7 %reduce-scatter.5.cloned.1.call-done = bf16[1024,512]{1,0:T(8,128)(2,1)} async-done(((bf16[1024,2048]{1,0:T(8,128)(2,1)}), bf16[1024,512]{1,0:T(8,128)(2,1)}) %reduce-scatter.5.cloned.1.call-update) | async-done | bytes 1048592 | tf_op jit(solution)/shard_map/reduce_scatter | solution.py:174
  (434 shorter events, 209.2 us)
Async XLA Ops:
  6.5 266.6 %copy-start = (bf16[512,2048]{1,0:T(8,128)(2,1)S(1)}, bf16[512,2048]{1,0:T(8,128)(2,1)}, u32[]{:S(2)}) copy-start(bf16[512,2048]{1,0:T(8,128)(2,1)} %param.35) | copy-start | bytes 6291460
  6.5 5.0 copy-start.10
  6.5 5.1 copy-start.11
  6.5 254.0 %all-gather.17.cloned.1.call-start = ((), (), s32[]{:S(2)}) async-start(), calls=%async_computation.7 | async-start | bytes 1179648 | tf_op jit(solution)/shard_map/all_gather | solution.py:16
  83.9 6.7 %copy-start.7 = (bf16[1024,256]{1,0:T(8,128)(2,1)S(1)}, bf16[1024,256]{1,0:T(8,128)(2,1)}, u32[]{:S(2)}) copy-start(bf16[1024,256]{1,0:T(8,128)(2,1)} %param.24) | copy-start | bytes 1572868
  84.6 180.5 %all-gather.15.cloned.1.call-start = ((), (), s32[]{:S(2)}) async-start(), calls=%async_computation.6 | async-start | bytes 2359296 | tf_op jit(solution)/shard_map/all_gather | solution.py:16
  91.6 8.2 %copy-start.8 = (bf16[1024,256]{1,0:T(8,128)(2,1)S(1)}, bf16[1024,256]{1,0:T(8,128)(2,1)}, u32[]{:S(2)}) copy-start(bf16[1024,256]{1,0:T(8,128)(2,1)} %param.25) | copy-start | bytes 1572868
  212.9 126.6 %reduce-scatter.3.cloned.1.call-start = ((), (), s32[]{:S(2)}) async-start(), calls=%async_computation.2 | async-start | bytes 5242880 | tf_op jit(solution)/shard_map/reduce_scatter | solution.py:155
  212.9 3.0 copy-start.3
  217.2 3.0 copy-start.4
  265.4 5.7 %copy-start.2 = (f32[1024,1,512]{0,2,1:T(8,128)S(1)}, f32[1024,1,512]{0,2,1:T(8,128)}, u32[]{:S(2)}) copy-start(f32[1024,1,512]{0,2,1:T(8,128)} %copy.34) | copy-start | bytes 6291460
  265.4 5.7 %copy-start.9 = (f32[16,64,1,128]{3,1,2,0:T(8,128)S(1)}, f32[16,64,1,128]{3,1,2,0:T(8,128)}, u32[]{:S(2)}) copy-start(f32[16,64,1,128]{3,1,2,0:T(8,128)} %get-tuple-element.194) | copy-start | bytes 1572868
  271.1 2.1 copy-start.6
  271.1 2.1 copy-start.13
  273.2 2.8 copy-start.5
  273.2 2.8 copy-start.12
  281.0 133.2 %all-gather.11.cloned.1.call-start = ((), (), s32[]{:S(2)}) async-start(), calls=%async_computation.3 | async-start | bytes 4718592 | tf_op jit(solution)/shard_map/all_gather | solution.py:128
  281.6 207.7 %all-gather.13.cloned.1.call-start = ((), (), s32[]{:S(2)}) async-start(), calls=%async_computation.4 | async-start | bytes 4718592 | tf_op jit(solution)/shard_map/all_gather | solution.py:129
  282.2 264.3 %reduce-scatter.5.cloned.1.call-start = ((), (), s32[]{:S(2)}) async-start(), calls=%async_computation.5 | async-start | bytes 5242880 | tf_op jit(solution)/shard_map/reduce_scatter | solution.py:174
  347.5 14.3 %collective-permute-start = (bf16[1024,512]{1,0:T(8,128)(2,1)S(1)}, bf16[1024,512]{1,0:T(8,128)(2,1)S(1)}, u32[]{:S(2)}, u32[]{:S(2)}) collective-permute-start(bf16[1024,512]{1,0:T(8,128)(2,1)S(1)} %fusion.75), channel_id=1, source_target_pairs={{0,1},{1,2},{2,3},{3,0},{4,5},{5,6},{6,7},{7,4},{8,9},{9,10},{10,1... | collective-permute-start | bytes 3145736 | tf_op jit(solution)/shard_map/ppermute | solution.py:167
  361.8 14.2 %collective-permute-start.1 = (bf16[1024,512]{1,0:T(8,128)(2,1)S(1)}, bf16[1024,512]{1,0:T(8,128)(2,1)S(1)}, u32[]{:S(2)}, u32[]{:S(2)}) collective-permute-start(bf16[1024,512]{1,0:T(8,128)(2,1)S(1)} %collective-permute-done), channel_id=1, source_target_pairs={{0,1},{1,2},{2,3},{3,0},{4,5},{5,6},{6,7},{7,4},{8,9},{9,10},{10,1... | collective-permute-start | bytes 3145736 | tf_op jit(solution)/shard_map/ppermute | solution.py:167
  376.0 14.3 %collective-permute-start.2 = (bf16[1024,512]{1,0:T(8,128)(2,1)S(1)}, bf16[1024,512]{1,0:T(8,128)(2,1)}, u32[]{:S(2)}, u32[]{:S(2)}) collective-permute-start(bf16[1024,512]{1,0:T(8,128)(2,1)S(1)} %collective-permute-done.1), channel_id=1, source_target_pairs={{0,1},{1,2},{2,3},{3,0},{4,5},{5,6},{6,7},{7,4},{8,9},{9,10},{10,1... | collective-permute-start | bytes 3145736 | tf_op jit(solution)/shard_map/ppermute | solution.py:167
  503.7 45.2 %copy-start.1 = (bf16[512,2048]{1,0:T(8,128)(2,1)S(1)}, bf16[512,2048]{1,0:T(8,128)(2,1)}, u32[]{:S(2)}) copy-start(bf16[512,2048]{1,0:T(8,128)(2,1)} %param.35) | copy-start | bytes 6291460
Sparse Core Ops, SparseCore 0:
  84.7 43.0 all-gather.16
  213.0 52.1 all-gather.14
  281.1 58.2 reduce-scatter.2
  341.4 72.7 all-gather.10
  416.1 73.1 all-gather.12
  503.8 42.5 reduce-scatter.4
